TPU v7x, 512 devices: a whole 4x4x16 slice. The times are simulated.
512 devices in a mesh: sp: 64 (over z, y), tp: 8 (over x, core).
Axes of the slice: x: 4, y: 4, z: 16, core: 2. Of those that a mesh axis runs over, the one named last changes fastest.
Arguments:
- residual: bfloat16 [8192, 2048], P('sp'), may hold values from -6 to 6
- query_nope: bfloat16 [8192, 8, 128], P('sp', 'tp'), may hold values from -6 to 6
- query_rope: bfloat16 [8192, 8, 64], P('sp', 'tp'), may hold values from -64 to 64
- latent: bfloat16 [8192, 256], P('sp'), may hold values from -6 to 6
- rope_key: bfloat16 [8192, 64], P('sp'), may hold values from -64 to 64
- kv_gain: bfloat16 [256], replicated, may hold values from 0.099609375 to 1.8984375
- key_up: bfloat16 [256, 8, 128], replicated, may hold values from -0.375 to 0.375
- value_up: bfloat16 [256, 8, 128], replicated, may hold values from -0.375 to 0.375
- out_weight: bfloat16 [1024, 2048], P('tp'), may hold values from -0.1875 to 0.1875
- post_gain: bfloat16 [2048], replicated, may hold values from 0.099609375 to 1.8984375
- pre_gain: bfloat16 [2048], replicated, may hold values from 0.099609375 to 1.8984375
- ffn_gain: bfloat16 [2048], replicated, may hold values from 0.099609375 to 1.8984375
- up_value: bfloat16 [2048, 5632], P('sp', 'tp'), may hold values from -0.125 to 0.125
- up_gate: bfloat16 [2048, 5632], P('sp', 'tp'), may hold values from -0.125 to 0.125
- conv_value: bfloat16 [3, 5632], replicated, may hold values from -3.5 to 3.5
- conv_gate: bfloat16 [3, 5632], replicated, may hold values from -3.5 to 3.5
- down_weight: bfloat16 [5632, 2048], P('tp', 'sp'), may hold values from -0.078125 to 0.078125
Outputs:
- layer_out: bfloat16 [8192, 2048], P(('sp', 'tp'))
All inputs are finite; a program needn't handle non-finite values.
Results may differ from a plain program's by a relative error of at most 0.02.
Values may be sent and summed in bfloat16 or wider, within the bound.
A program may use at most 128 MiB of HBM per device.

v0:
```python
import jax
import jax.numpy as jnp
from jax import lax
from jax.sharding import Mesh
from jax.sharding import PartitionSpec as P

GRID = 64
SP = ("sp_0", "sp_1")
SP_TP = ("sp_0", "sp_1", "tp")
epsilon = 1e-06
rope_base = 10000.0


def side_by_side(arrays, axis, dim, along):
    both = jnp.concatenate(arrays, axis=along)
    whole, at, outs = (lax.all_gather(both, axis, axis=dim, tiled=True), 0, [])
    for a in arrays:
        outs.append(lax.slice_in_dim(whole, at, at + a.shape[along], axis=along))
        at += a.shape[along]
    return tuple(outs)


def sent_to_all(x, axis):
    size = lax.axis_size(axis)
    return lax.all_to_all(jnp.broadcast_to(x[None], (size, *x.shape)), axis, 0, 0, tiled=True)


def taken_together(x, axis):
    return sent_to_all(x, axis).astype(jnp.float32).sum(axis=0)


def joined_along(pieces, dim):
    pieces = jnp.moveaxis(pieces, 0, dim)
    shape = pieces.shape
    return pieces.reshape(*shape[:dim], shape[dim] * shape[dim + 1], *shape[dim + 2 :])


def stacked_from(x, axes, order):
    pieces = x[None]
    for k in order:
        pieces = lax.all_gather(pieces, axes[k], axis=0, tiled=True)
    current = [lax.axis_size(axes[k]) for k in reversed(order)]
    pieces = pieces.reshape(*current, *x.shape)
    turned = sorted(range(len(order)), key=lambda place: order[len(order) - 1 - place])
    return pieces.transpose(*turned, *range(len(order), pieces.ndim)).reshape(-1, *x.shape)


def gathered_by_axis(x, axes, order, dim):
    return joined_along(stacked_from(x, axes, order), dim)


def extended(x, sides, width):
    for axis, dim in sides:
        size, length = (lax.axis_size(axis), x.shape[dim])
        up = [(i, (i + 1) % size) for i in range(size - 1)]
        down = [(j, i) for i, j in up]
        last = lax.slice_in_dim(x, length - width, length, axis=dim)
        initial = lax.slice_in_dim(x, 0, width, axis=dim)
        before = lax.ppermute(last, axis, up)
        after = lax.ppermute(initial, axis, down)
        x = jnp.concatenate([before, x, after], axis=dim)
    return x


def whole_of(x, axes, dim):
    for axis in reversed(axes):
        x = lax.all_gather(x, axis, axis=dim, tiled=True)
    return x


def split_up(x, dim, size):
    shape = x.shape
    pieces = x.reshape(*shape[:dim], size, shape[dim] // size, *shape[dim + 1 :])
    return jnp.moveaxis(pieces, dim, 0)


def sum_at_owner(x, axis, dim):
    size = lax.axis_size(axis)
    pieces = lax.all_to_all(split_up(x, dim, size), axis, 0, 0, tiled=True)
    return jnp.sum(pieces.astype(jnp.float32), axis=0)


def rms_norm(values, gain):
    return (
        values
        * lax.rsqrt(jnp.mean(values * values, axis=-1, keepdims=True) + epsilon)
        * gain.astype(jnp.float32)
    )


def widened(values):
    return lax.optimization_barrier(values.astype(jnp.bfloat16)).astype(jnp.float32)


def rotate(values, positions):
    pair_count = values.shape[-1] // 4
    frequency = rope_base ** (-jnp.arange(pair_count, dtype=jnp.float32) / pair_count)
    grid_rows = (positions // GRID).astype(jnp.float32)
    grid_cols = (positions % GRID).astype(jnp.float32)
    angles = jnp.stack([grid_rows, grid_cols], axis=-1)[:, :, None] * frequency
    table_shape = (angles.shape[0],) + (1,) * (values.ndim - 2) + angles.shape[1:]
    cosine = jnp.cos(angles).reshape(table_shape)
    sine = jnp.sin(angles).reshape(table_shape)
    halves = values.reshape(values.shape[:-1] + (2, 2, pair_count))
    leading = halves[..., 0, :]
    trailing = halves[..., 1, :]
    turned = jnp.stack(
        [leading * cosine - trailing * sine, trailing * cosine + leading * sine], axis=-2
    )
    return turned.reshape(values.shape)


def body(
    residual,
    query_nope,
    query_rope,
    latent,
    rope_key,
    kv_gain,
    key_up,
    value_up,
    out_weight,
    post_gain,
    pre_gain,
    ffn_gain,
    up_value,
    up_gate,
    conv_value,
    conv_gate,
    down_weight,
):
    tok_rows = residual.shape[0]
    heads_dev = query_nope.shape[1]
    value_width = value_up.shape[2]
    tp_index = lax.axis_index("tp")
    positions = lax.axis_index(SP) * tok_rows + jnp.arange(tok_rows, dtype=jnp.int32)
    score_scale = (query_nope.shape[2] + query_rope.shape[2]) ** (-0.5)
    normed = rms_norm(latent.astype(jnp.float32), kv_gain).astype(jnp.bfloat16)
    key_turn = rotate(rope_key.astype(jnp.float32), positions).astype(jnp.bfloat16)
    query_turn = rotate(query_rope.astype(jnp.float32), positions).astype(jnp.bfloat16)
    key_local = lax.dynamic_slice_in_dim(key_up, tp_index * heads_dev, heads_dev, 1)
    value_local = lax.dynamic_slice_in_dim(value_up, tp_index * heads_dev, heads_dev, 1)
    pieces = side_by_side((normed, key_turn), SP, 0, 1)
    keys_nope = jnp.einsum(
        "nc,chd->nhd", pieces[0], key_local, preferred_element_type=jnp.float32
    ).astype(jnp.bfloat16)
    values_part = jnp.einsum(
        "nc,chd->nhd", pieces[0], value_local, preferred_element_type=jnp.float32
    ).astype(jnp.bfloat16)
    row_max = jnp.full((heads_dev, tok_rows), -1e30, jnp.float32)
    scores = (
        jnp.einsum("qhd,khd->hqk", query_nope, keys_nope, preferred_element_type=jnp.float32)
        + jnp.einsum("qhd,kd->hqk", query_turn, pieces[1], preferred_element_type=jnp.float32)
    ) * score_scale
    new_max = jnp.maximum(row_max, jnp.max(scores, axis=-1))
    weights = jnp.exp(scores - new_max[:, :, None])
    totals = jnp.sum(weights, axis=-1)
    weighted = jnp.einsum(
        "hqk,khd->hqd",
        weights.astype(jnp.bfloat16),
        values_part,
        preferred_element_type=jnp.float32,
    )
    attended = (weighted / totals[:, :, None]).astype(jnp.bfloat16)
    attended = jnp.transpose(attended, (1, 0, 2)).reshape(tok_rows, heads_dev * value_width)
    row_share = tok_rows // lax.axis_size("tp")
    summed = taken_together(
        jnp.dot(attended, out_weight, preferred_element_type=jnp.float32).astype(jnp.bfloat16), "tp"
    ).astype(jnp.float32)
    stream_all = widened(residual.astype(jnp.float32) + rms_norm(widened(summed), post_gain))
    inputs = rms_norm(stream_all, pre_gain).astype(jnp.bfloat16)
    stream_wide = lax.dynamic_slice_in_dim(stream_all, tp_index * row_share, row_share, 0)
    ff_dev = up_value.shape[1]
    up_joined = jnp.concatenate([up_value, up_gate], axis=1)
    up_whole = gathered_by_axis(up_joined, SP, (0, 1), 0)
    up_pair = jnp.dot(inputs, up_whole, preferred_element_type=jnp.float32).astype(jnp.bfloat16)
    padded = extended(up_pair, ((SP, 0),), 1).astype(jnp.float32)
    channel_start = tp_index * ff_dev
    conv_taps = jnp.concatenate(
        [
            lax.dynamic_slice_in_dim(conv_value, channel_start, ff_dev, 1),
            lax.dynamic_slice_in_dim(conv_gate, channel_start, ff_dev, 1),
        ],
        axis=1,
    ).astype(jnp.float32)
    mixed_conv = (
        padded[:-2] * conv_taps[0] + padded[1:-1] * conv_taps[1] + padded[2:] * conv_taps[2]
    )
    hidden = (jax.nn.silu(mixed_conv[:, ff_dev:]) * mixed_conv[:, :ff_dev]).astype(jnp.bfloat16)
    down_whole = whole_of(down_weight, SP, 1)
    down_terms = jnp.dot(hidden, down_whole, preferred_element_type=jnp.float32)
    reduced = sum_at_owner(down_terms.astype(jnp.bfloat16), "tp", 0)
    return (stream_wide + rms_norm(widened(reduced), ffn_gain)).astype(jnp.bfloat16)


def solution(mesh):
    torus = Mesh(mesh.devices.reshape(16, 4, mesh.shape["tp"]), ("sp_0", "sp_1", "tp"))
    return jax.shard_map(
        body,
        mesh=torus,
        in_specs=(
            P(SP, None),
            P(SP, "tp", None),
            P(SP, "tp", None),
            P(SP, None),
            P(SP, None),
            P(),
            P(),
            P(),
            P("tp", None),
            P(),
            P(),
            P(),
            P(SP, "tp"),
            P(SP, "tp"),
            P(),
            P(),
            P("tp", SP),
        ),
        out_specs=P(SP_TP, None),
        check_vma=False,
    )
```

profile of v0, /device:TPU:1, one launch (start us, length us, event | category | flops | bytes accessed | tf_op | source)
XLA Modules:
  0.0 408.5 jit_solution(6371514957831806207)
XLA Ops:
  6.5 1.6 pad_maximum_fusion.1
  9.9 0.9 fusion.37
  12.6 64.1 %all-gather.12.cloned.1.call-done = bf16[512,1408]{1,0:T(8,128)(2,1)} async-done(((bf16[32,1408]{1,0:T(8,128)(2,1)}), bf16[512,1408]{1,0:T(8,128)(2,1)}) %all-gather.12.cloned.1.call-update) | async-done | bytes 1441808 | tf_op jit(solution)/shard_map/all_gather | solution.py:41
  77.6 1.5 constant_dynamic-slice_fusion.2
  79.1 149.7 %all-gather.6.cloned.1.call-done = bf16[8192,320]{1,0:T(8,128)(2,1)} async-done(((bf16[128,320]{1,0:T(8,128)(2,1)}), bf16[8192,320]{1,0:T(8,128)(2,1)}) %all-gather.6.cloned.1.call-update) | async-done | bytes 5242896 | tf_op jit(solution)/shard_map/all_gather | solution.py:16
  228.8 4.2 %convolution_bitcast_fusion = f32[1,128,8192]{1,2,0:T(8,128)} fusion(bf16[128,64]{0,1:T(8,128)(2,1)S(1)} %bitcast.54, bf16[8192,320]{1,0:T(8,128)(2,1)} %all-gather.6.cloned.1.call-done), kind=kOutput, calls=%fused_computation | convolution fusion | flops 134217728 | bytes 6307840 | tf_op jit(solution)/shard_map/qhd,kd->hqk/dot_general | solution.py:153
  233.0 7.6 %fusion.67 = (f32[128]{0:T(128)S(1)}, f32[1,128,8192]{1,2,0:T(8,128)}) fusion(f32[1,128,8192]{1,2,0:T(8,128)} %convolution_bitcast_fusion, bf16[128,1,128]{2,0,1:T(8,128)(2,1)S(1)} %copy-done.3, bf16[8192,320]{1,0:T(8,128)(2,1)} %all-gather.6.cloned.1.call-done, bf16[256,1,128]{2,1,0:T(2,128)(2,1)S(1)} %get-tuple-element.19), kind=kOutput, calls=%fused_computation.104 | convolution fusion | flops 809500544 | bytes 12681728 | tf_op jit(solution)/shard_map/qhd,khd->hqk/dot_general | solution.py:152
  240.6 3.3 fusion.2
  243.8 5.7 %fusion.20 = bf16[128,128]{1,0:T(8,128)(2,1)S(1)} fusion(bf16[8192,320]{1,0:T(8,128)(2,1)} %all-gather.6.cloned.1.call-done, f32[1,128,8192]{1,2,0:T(8,128)} %get-tuple-element.15, f32[128]{0:T(128)S(1)} %broadcast_maximum_fusion, bf16[256,1,128]{2,1,0:T(2,128)(2,1)S(1)} %get-tuple-element.18, f32[128]{0:T(128)S(1)} %fusion.2), kind=kOutput, calls=%fused_computation.21 | convolution fusion | flops 808484864 | bytes 8487936 | tf_op jit(solution)/shard_map/hqk,khd->hqd/dot_general | solution.py:158
  249.9 2.5 broadcast_in_dim.7
  252.4 14.1 %all-to-all-start = ((bf16[8,128,2048]{2,1,0:T(8,128)(2,1)}), bf16[8,128,2048]{2,1,0:T(8,128)(2,1)}, u32[]{:S(2)}, u32[]{:S(2)}) async-start(bf16[8,128,2048]{2,1,0:T(8,128)(2,1)} %broadcast_in_dim.7), calls=%async_computation | async-start | bytes 8388608 | tf_op jit(solution)/shard_map/all_to_all | solution.py:25
  266.5 12.0 %all_gather.18 = bf16[704,128]{0,1:T(8,128)(2,1)} all-gather(bf16[704,32]{0,1:T(8,128)(2,1)S(1)} %copy-done.2), channel_id=1, replica_groups=mesh['sp_0'=16,'sp_1'=4,'tp'=8] {'sp_1'}, dimensions={1}, use_global_device_ids=true | all-gather | bytes 225280 | tf_op jit(solution)/shard_map/all_gather | solution.py:67
  279.3 25.3 %all-gather.8.cloned.1.call-done = bf16[64,32,1408]{2,1,0:T(8,128)(2,1)} async-done(((bf16[16,32,1408]{2,1,0:T(8,128)(2,1)}), bf16[64,32,1408]{2,1,0:T(8,128)(2,1)}) %all-gather.8.cloned.1.call-update) | async-done | bytes 5767184 | tf_op jit(solution)/shard_map/all_gather | solution.py:41
  304.7 5.8 %copy.33 = bf16[16,4,32,1408]{3,2,1,0:T(8,128)(2,1)} copy(bf16[16,4,32,1408]{3,2,0,1:T(8,128)(2,1)} %bitcast.52) | data formatting | bytes 11534336 | tf_op jit(solution)/shard_map/transpose | solution.py:45
  310.5 4.7 %all-to-all-done = bf16[8,128,2048]{2,1,0:T(8,128)(2,1)} async-done(((bf16[8,128,2048]{2,1,0:T(8,128)(2,1)}), bf16[8,128,2048]{2,1,0:T(8,128)(2,1)}, u32[]{:S(2)}, u32[]{:S(2)}) %all-to-all-start) | async-done | bytes 4194336 | tf_op jit(solution)/shard_map/all_to_all | solution.py:25
  315.3 3.0 reduce_sum.71
  318.9 3.7 convolution_convert_fusion.4
  322.6 2.5 collective-permute-start
  325.1 1.3 collective-permute-start.1
  326.5 3.3 collective-permute-done.1
  330.2 43.6 %all-gather.10.cloned.1.call-done = bf16[704,2048]{0,1:T(8,128)(2,1)} async-done(((bf16[704,128]{0,1:T(8,128)(2,1)}), bf16[704,2048]{0,1:T(8,128)(2,1)}) %all-gather.10.cloned.1.call-update) | async-done | bytes 2883600 | tf_op jit(solution)/shard_map/all_gather | solution.py:67
  373.8 3.9 convolution_convert_fusion.2
  377.6 14.0 %all-to-all-start.1 = ((bf16[8,16,2048]{2,1,0:T(8,128)(2,1)}), bf16[8,16,2048]{2,1,0:T(8,128)(2,1)S(1)}, u32[]{:S(2)}, u32[]{:S(2)}) async-start(bf16[8,16,2048]{2,1,0:T(8,128)(2,1)} %bitcast.18), calls=%async_computation.1 | async-start | bytes 1048576 | tf_op jit(solution)/shard_map/all_to_all | solution.py:79
  391.8 9.2 %all-to-all-done.1 = bf16[8,16,2048]{2,1,0:T(8,128)(2,1)S(1)} async-done(((bf16[8,16,2048]{2,1,0:T(8,128)(2,1)}), bf16[8,16,2048]{2,1,0:T(8,128)(2,1)S(1)}, u32[]{:S(2)}, u32[]{:S(2)}) %all-to-all-start.1) | async-done | bytes 524320 | tf_op jit(solution)/shard_map/all_to_all | solution.py:79
  (57 shorter events, 7.6 us)
Async XLA Ops:
  6.5 243.0 %copy-start = (bf16[128,2048]{1,0:T(8,128)(2,1)S(1)}, bf16[128,2048]{1,0:T(8,128)(2,1)}, u32[]{:S(2)}) copy-start(bf16[128,2048]{1,0:T(8,128)(2,1)} %param.25) | copy-start | bytes 1572868
  6.5 70.1 %all-gather.12.cloned.1.call-start = ((), (), s32[]{:S(2)}) async-start(), calls=%async_computation.5 | async-start | bytes 1531904 | tf_op jit(solution)/shard_map/all_gather | solution.py:41
  8.2 220.6 %all-gather.6.cloned.1.call-start = ((), (), s32[]{:S(2)}) async-start(), calls=%async_computation.2 | async-start | bytes 6389760 | tf_op jit(solution)/shard_map/all_gather | solution.py:16
  12.5 292.2 %all-gather.8.cloned.1.call-start = ((), (), s32[]{:S(2)}) async-start(), calls=%async_computation.3 | async-start | bytes 7208960 | tf_op jit(solution)/shard_map/all_gather | solution.py:41
  77.6 155.4 %copy-start.3 = (bf16[128,1,128]{2,0,1:T(8,128)(2,1)S(1)}, bf16[128,1,128]{2,0,1:T(8,128)(2,1)}, u32[]{:S(2)}) copy-start(bf16[128,1,128]{2,0,1:T(8,128)(2,1)} %param.18) | copy-start | bytes 98308
  252.4 14.1 %copy-start.2 = (bf16[704,32]{0,1:T(8,128)(2,1)S(1)}, bf16[704,32]{0,1:T(8,128)(2,1)}, u32[]{:S(2)}) copy-start(bf16[704,32]{0,1:T(8,128)(2,1)} %param.33) | copy-start | bytes 135172
  252.4 26.1 %copy-start.4 = (bf16[2048]{0:T(1024)(128)(2,1)S(1)}, bf16[2048]{0:T(1024)(128)(2,1)}, u32[]{:S(2)}) copy-start(bf16[2048]{0:T(1024)(128)(2,1)} %param.26) | copy-start | bytes 12292
  252.4 26.1 %copy-start.5 = (bf16[2048]{0:T(1024)(128)(2,1)S(1)}, bf16[2048]{0:T(1024)(128)(2,1)}, u32[]{:S(2)}) copy-start(bf16[2048]{0:T(1024)(128)(2,1)} %param.27) | copy-start | bytes 12292
  252.4 62.9 %all-to-all-start = ((bf16[8,128,2048]{2,1,0:T(8,128)(2,1)}), bf16[8,128,2048]{2,1,0:T(8,128)(2,1)}, u32[]{:S(2)}, u32[]{:S(2)}) async-start(bf16[8,128,2048]{2,1,0:T(8,128)(2,1)} %broadcast_in_dim.7), calls=%async_computation | async-start | bytes 8388608 | tf_op jit(solution)/shard_map/all_to_all | solution.py:25
  266.4 107.3 %all-gather.10.cloned.1.call-start = ((), (), s32[]{:S(2)}) async-start(), calls=%async_computation.4 | async-start | bytes 3342336 | tf_op jit(solution)/shard_map/all_gather | solution.py:67
  310.5 7.9 %copy-start.1 = (bf16[128,2048]{1,0:T(8,128)(2,1)S(1)}, bf16[128,2048]{1,0:T(8,128)(2,1)}, u32[]{:S(2)}) copy-start(bf16[128,2048]{1,0:T(8,128)(2,1)} %param.17) | copy-start | bytes 1572868
  322.6 3.9 collective-permute-start
  325.1 4.8 %collective-permute-start.1 = (bf16[1,1408]{1,0:T(2,128)(2,1)S(1)}, bf16[1,1408]{1,0:T(2,128)(2,1)S(1)}, u32[]{:S(2)}, u32[]{:S(2)}) collective-permute-start(bf16[1,1408]{1,0:T(2,128)(2,1)S(1)} %get-tuple-element.9), channel_id=1, source_target_pairs={{8,0},{16,8},{24,16},{32,24},{40,32},{48,40},{56,48},{64,56},{72,6... | collective-permute-start | bytes 8456 | tf_op jit(solution)/shard_map/ppermute | solution.py:60
  330.0 61.7 %copy-start.6 = (bf16[2048]{0:T(1024)(128)(2,1)S(1)}, bf16[2048]{0:T(1024)(128)(2,1)}, u32[]{:S(2)}) copy-start(bf16[2048]{0:T(1024)(128)(2,1)} %param.28) | copy-start | bytes 12292
  377.6 23.4 %all-to-all-start.1 = ((bf16[8,16,2048]{2,1,0:T(8,128)(2,1)}), bf16[8,16,2048]{2,1,0:T(8,128)(2,1)S(1)}, u32[]{:S(2)}, u32[]{:S(2)}) async-start(bf16[8,16,2048]{2,1,0:T(8,128)(2,1)} %bitcast.18), calls=%async_computation.1 | async-start | bytes 1048576 | tf_op jit(solution)/shard_map/all_to_all | solution.py:79
Sparse Core Ops, SparseCore 0:
  9.4 67.2 all-gather.11
  79.6 149.0 all-gather.5
  230.9 73.7 all-gather.7
  306.6 67.1 all-gather.9
where the time goes:
time: 409 us; the launch traced here: 408 us
  waiting for transfers between devices  300 us (73%)
  starting transfers between devices  32 us (8%)
  matrix products  25.3 us (6%)
  other arithmetic  15 us (4%)
  between operations  13.3 us (3%)
  blocking collectives  12 us (3%)
  local copies, waits for them, and re-layouts  10.8 us (3%)
    all_gather x1, waiting for transfers between devices, side_by_side(): whole, at, outs = (lax.all_gather(both, axis, axis=dim, tiled=True), 0, [])  150 us
    all_gather x2, waiting for transfers between devices, stacked_from(): pieces = lax.all_gather(pieces, axes[k], axis=0, tiled=True)  89.5 us
    all_gather x1, waiting for transfers between devices, whole_of(): x = lax.all_gather(x, axis, axis=dim, tiled=True)  43.6 us
    all_to_all x1, starting transfers between devices, sent_to_all(): lax.all_to_all(jnp.broadcast_to(x[None], (size, *x.shape)), axis, 0, 0, t...  14.1 us
    all_to_all x1, starting transfers between devices, sum_at_owner(): pieces = lax.all_to_all(split_up(x, dim, size), axis, 0, 0, tiled=True)  14 us
    all_gather x1, blocking collectives, whole_of(): x = lax.all_gather(x, axis, axis=dim, tiled=True)  12 us
    all_to_all x1, waiting for transfers between devices, sum_at_owner(): pieces = lax.all_to_all(split_up(x, dim, size), axis, 0, 0, tiled=True)  9.23 us
  transfers between devices with their start and end apart: 8, of which 7 were waited for; matrix products, arithmetic and copies ran while one was open for 11% of the time, Pallas kernels for 0%

commit v1 on v0

--- a/solution.py
+++ b/solution.py
@@ -38,7 +38,9 @@
 def stacked_from(x, axes, order):
     pieces = x[None]
     for k in order:
-        pieces = lax.all_gather(pieces, axes[k], axis=0, tiled=True)
+        pieces = jnp.concatenate(
+            lax.all_to_all(jnp.stack([pieces] * lax.axis_size(axes[k])), axes[k], 0, 0), axis=0
+        )
     current = [lax.axis_size(axes[k]) for k in reversed(order)]
     pieces = pieces.reshape(*current, *x.shape)
     turned = sorted(range(len(order)), key=lambda place: order[len(order) - 1 - place])

time: 409 us -> 364 us (0.89)
  waiting for transfers between devices: 300 us -> 169 us
  blocking collectives: 12 us -> 94.6 us
    all_gather x2 -> x0, waiting for transfers between devices: 89.5 us -> none  [stacked_from(): pieces = lax.all_gather(pieces, axes[k], axis=0, tiled=True)]
    all_to_all x0 -> x1, blocking collectives: none -> 83.7 us  [stacked_from(): lax.all_to_all(jnp.stack([pieces] * lax.axis_size(axes[k])), axes[k], 0, 0)]
    all_gather x1, waiting for transfers between devices: 150 us -> 113 us  [side_by_side(): whole, at, outs = (lax.all_gather(both, axis, axis=dim, tiled=True), 0, [])]
    all_gather x1, waiting for transfers between devices: 43.6 us -> 12.4 us  [whole_of(): x = lax.all_gather(x, axis, axis=dim, tiled=True)]
    all_to_all x1, waiting for transfers between devices: 4.73 us -> 31.1 us  [sent_to_all(): lax.all_to_all(jnp.broadcast_to(x[None], (size, *x.shape)), axis, 0, 0, t...]
    all_to_all x0 -> x1, local copies, waits for them, and re-layouts: none -> 5.89 us  [stacked_from(): lax.all_to_all(jnp.stack([pieces] * lax.axis_size(axes[k])), axes[k], 0, 0)]
    transpose x1 -> x0, local copies, waits for them, and re-layouts: 5.83 us -> none  [stacked_from(): pieces.transpose(*turned, *range(len(order), pieces.ndim))]
    all_to_all x0 -> x1, starting transfers between devices: none -> 5.28 us  [stacked_from(): lax.all_to_all(jnp.stack([pieces] * lax.axis_size(axes[k])), axes[k], 0, 0)]
  transfers between devices with their start and end apart: 8 -> 7, of which waited for: 7 -> 5; matrix products, arithmetic and copies ran while one was open for 11% -> 11% of each run, Pallas kernels for 0% -> 0%
where the time goes in v1:
time: 364 us; the launch traced here: 363 us
  waiting for transfers between devices  169 us (46%)
  blocking collectives  94.6 us (26%)
  starting transfers between devices  31.3 us (9%)
  matrix products  25.5 us (7%)
  between operations  15.1 us (4%)
  local copies, waits for them, and re-layouts  14 us (4%)
  other arithmetic  13.6 us (4%)
    all_gather x1, waiting for transfers between devices, side_by_side(): whole, at, outs = (lax.all_gather(both, axis, axis=dim, tiled=True), 0, [])  113 us
    all_to_all x1, blocking collectives, stacked_from(): lax.all_to_all(jnp.stack([pieces] * lax.axis_size(axes[k])), axes[k], 0, 0)  83.7 us
    all_to_all x1, waiting for transfers between devices, sent_to_all(): lax.all_to_all(jnp.broadcast_to(x[None], (size, *x.shape)), axis, 0, 0, t...  31.1 us
    all_to_all x1, starting transfers between devices, sum_at_owner(): pieces = lax.all_to_all(split_up(x, dim, size), axis, 0, 0, tiled=True)  13.7 us
    all_gather x1, waiting for transfers between devices, whole_of(): x = lax.all_gather(x, axis, axis=dim, tiled=True)  12.4 us
    all_gather x1, blocking collectives, whole_of(): x = lax.all_gather(x, axis, axis=dim, tiled=True)  10.9 us
    all_to_all x1, starting transfers between devices, sent_to_all(): lax.all_to_all(jnp.broadcast_to(x[None], (size, *x.shape)), axis, 0, 0, t...  9.77 us
    all_to_all x1, waiting for transfers between devices, sum_at_owner(): pieces = lax.all_to_all(split_up(x, dim, size), axis, 0, 0, tiled=True)  9.23 us
  transfers between devices with their start and end apart: 7, of which 5 were waited for; matrix products, arithmetic and copies ran while one was open for 11% of the time, Pallas kernels for 0%

profile of v1, /device:TPU:1, one launch (start us, length us, event | category | flops | bytes accessed | tf_op | source)
XLA Modules:
  0.0 363.1 jit_solution(6099380390669855750)
XLA Ops:
  8.5 1.0 fusion.37
  12.7 83.7 %all_to_all.20 = bf16[16,1,32,1408]{3,2,1,0:T(8,128)(2,1)S(1)} all-to-all(bf16[16,1,32,1408]{3,2,1,0:T(8,128)(2,1)S(1)} %stack.29), channel_id=1, replica_groups=mesh['sp_0'=16,'sp_1'=4,'tp'=8] {'sp_0'}, dimensions={0} | all-to-all | bytes 2883584 | tf_op jit(solution)/shard_map/all_to_all | solution.py:42
  96.4 3.1 stack.30
  99.5 5.3 %all-to-all-start.2 = ((bf16[4,16,32,1408]{3,2,1,0:T(8,128)(2,1)}), bf16[4,16,32,1408]{3,2,1,0:T(8,128)(2,1)}, u32[]{:S(2)}, u32[]{:S(2)}) async-start(bf16[4,16,32,1408]{3,2,1,0:T(8,128)(2,1)} %stack.30), calls=%async_computation.2 | async-start | bytes 11534336 | tf_op jit(solution)/shard_map/all_to_all | solution.py:42
  105.0 1.5 constant_dynamic-slice_fusion.2
  106.5 112.8 %all-gather.3.cloned.1.call-done = bf16[8192,320]{1,0:T(8,128)(2,1)} async-done(((bf16[128,320]{1,0:T(8,128)(2,1)}), bf16[8192,320]{1,0:T(8,128)(2,1)}) %all-gather.3.cloned.1.call-update) | async-done | bytes 5242896 | tf_op jit(solution)/shard_map/all_gather | solution.py:16
  219.3 4.3 %convolution_bitcast_fusion = f32[1,128,8192]{1,2,0:T(8,128)} fusion(bf16[128,64]{0,1:T(8,128)(2,1)S(1)} %bitcast.52, bf16[8192,320]{1,0:T(8,128)(2,1)} %all-gather.3.cloned.1.call-done), kind=kOutput, calls=%fused_computation | convolution fusion | flops 134217728 | bytes 6307840 | tf_op jit(solution)/shard_map/qhd,kd->hqk/dot_general | solution.py:155
  223.6 7.7 %fusion.67 = (f32[128]{0:T(128)S(1)}, f32[1,128,8192]{1,2,0:T(8,128)}) fusion(f32[1,128,8192]{1,2,0:T(8,128)} %convolution_bitcast_fusion, bf16[128,1,128]{2,0,1:T(8,128)(2,1)S(1)} %copy-done.3, bf16[8192,320]{1,0:T(8,128)(2,1)} %all-gather.3.cloned.1.call-done, bf16[256,1,128]{2,1,0:T(2,128)(2,1)S(1)} %get-tuple-element.19), kind=kOutput, calls=%fused_computation.104 | convolution fusion | flops 809500544 | bytes 12681728 | tf_op jit(solution)/shard_map/qhd,khd->hqk/dot_general | solution.py:154
  231.2 3.3 fusion.2
  234.5 5.7 %fusion.20 = bf16[128,128]{1,0:T(8,128)(2,1)S(1)} fusion(bf16[8192,320]{1,0:T(8,128)(2,1)} %all-gather.3.cloned.1.call-done, f32[1,128,8192]{1,2,0:T(8,128)} %get-tuple-element.15, f32[128]{0:T(128)S(1)} %broadcast_maximum_fusion, bf16[256,1,128]{2,1,0:T(2,128)(2,1)S(1)} %get-tuple-element.18, f32[128]{0:T(128)S(1)} %fusion.2), kind=kOutput, calls=%fused_computation.21 | convolution fusion | flops 808484864 | bytes 8487936 | tf_op jit(solution)/shard_map/hqk,khd->hqd/dot_general | solution.py:160
  240.6 2.5 broadcast_in_dim.5
  243.0 9.8 %all-to-all-start = ((bf16[8,128,2048]{2,1,0:T(8,128)(2,1)}), bf16[8,128,2048]{2,1,0:T(8,128)(2,1)}, u32[]{:S(2)}, u32[]{:S(2)}) async-start(bf16[8,128,2048]{2,1,0:T(8,128)(2,1)} %broadcast_in_dim.5), calls=%async_computation | async-start | bytes 8388608 | tf_op jit(solution)/shard_map/all_to_all | solution.py:25
  252.8 10.9 %all_gather.10 = bf16[704,128]{0,1:T(8,128)(2,1)} all-gather(bf16[704,32]{0,1:T(8,128)(2,1)S(1)} %copy-done.2), channel_id=1, replica_groups=mesh['sp_0'=16,'sp_1'=4,'tp'=8] {'sp_1'}, dimensions={1}, use_global_device_ids=true | all-gather | bytes 225280 | tf_op jit(solution)/shard_map/all_gather | solution.py:69
  264.6 5.9 %copy.29 = bf16[4,16,32,1408]{3,2,0,1:T(8,128)(2,1)} copy(bf16[4,16,32,1408]{3,2,1,0:T(8,128)(2,1)} %all-to-all-done.2) | data formatting | bytes 11534336 | tf_op jit(solution)/shard_map/all_to_all | solution.py:42
  270.5 31.1 %all-to-all-done = bf16[8,128,2048]{2,1,0:T(8,128)(2,1)} async-done(((bf16[8,128,2048]{2,1,0:T(8,128)(2,1)}), bf16[8,128,2048]{2,1,0:T(8,128)(2,1)}, u32[]{:S(2)}, u32[]{:S(2)}) %all-to-all-start) | async-done | bytes 4194336 | tf_op jit(solution)/shard_map/all_to_all | solution.py:25
  301.6 3.0 reduce_sum.71
  305.3 3.7 %convolution_convert_fusion.4 = bf16[128,1408]{1,0:T(8,128)(2,1)S(1)} fusion(bf16[2048,1408]{1,0:T(8,128)(2,1)} %bitcast.50, f32[2048]{0:T(1024)S(1)} %convert_element_type.128, f32[128]{0:T(128)S(1)} %add_rsqrt_fusion.1, bf16[128,2048]{1,0:T(8,128)(2,1)S(1)} %fusion.28), kind=kOutput, calls=%fused_computation.13 | convolution fusion | flops 739426304 | bytes 6660608 | tf_op jit(solution)/shard_map/dot_general | solution.py:178
  309.0 1.3 collective-permute-start
  310.3 1.3 collective-permute-start.1
  311.7 3.3 collective-permute-done.1
  315.4 12.4 %all-gather.5.cloned.1.call-done = bf16[704,2048]{0,1:T(8,128)(2,1)} async-done(((bf16[704,128]{0,1:T(8,128)(2,1)}), bf16[704,2048]{0,1:T(8,128)(2,1)}) %all-gather.5.cloned.1.call-update) | async-done | bytes 2883600 | tf_op jit(solution)/shard_map/all_gather | solution.py:69
  327.8 3.9 %convolution_convert_fusion.2 = bf16[128,2048]{1,0:T(8,128)(2,1)} fusion(bf16[704,2048]{0,1:T(8,128)(2,1)} %all-gather.5.cloned.1.call-done, f32[128,1408]{1,0:T(8,128)S(1)} %fusion.29), kind=kOutput, calls=%fused_computation.11 | convolution fusion | flops 369901568 | bytes 4194304 | tf_op jit(solution)/shard_map/dot_general | solution.py:193
  331.7 13.7 %all-to-all-start.3 = ((bf16[8,16,2048]{2,1,0:T(8,128)(2,1)}), bf16[8,16,2048]{2,1,0:T(8,128)(2,1)S(1)}, u32[]{:S(2)}, u32[]{:S(2)}) async-start(bf16[8,16,2048]{2,1,0:T(8,128)(2,1)} %bitcast.17), calls=%async_computation.3 | async-start | bytes 1048576 | tf_op jit(solution)/shard_map/all_to_all | solution.py:81
  345.5 9.2 %all-to-all-done.3 = bf16[8,16,2048]{2,1,0:T(8,128)(2,1)S(1)} async-done(((bf16[8,16,2048]{2,1,0:T(8,128)(2,1)}), bf16[8,16,2048]{2,1,0:T(8,128)(2,1)S(1)}, u32[]{:S(2)}, u32[]{:S(2)}) %all-to-all-start.3) | async-done | bytes 524320 | tf_op jit(solution)/shard_map/all_to_all | solution.py:81
  (58 shorter events, 7.8 us)
Async XLA Ops:
  7.4 232.9 %copy-start = (bf16[128,2048]{1,0:T(8,128)(2,1)S(1)}, bf16[128,2048]{1,0:T(8,128)(2,1)}, u32[]{:S(2)}) copy-start(bf16[128,2048]{1,0:T(8,128)(2,1)} %param.25) | copy-start | bytes 1572868
  7.4 211.9 %all-gather.3.cloned.1.call-start = ((), (), s32[]{:S(2)}) async-start(), calls=%async_computation.4 | async-start | bytes 6389760 | tf_op jit(solution)/shard_map/all_gather | solution.py:16
  99.5 5.3 %copy-start.4 = (bf16[128,1,64]{0,2,1:T(8,128)(2,1)S(1)}, bf16[128,1,64]{0,2,1:T(8,128)(2,1)}, u32[]{:S(2)}) copy-start(bf16[128,1,64]{0,2,1:T(8,128)(2,1)} %param.19) | copy-start | bytes 49156
  99.5 141.0 %all-to-all-start.2 = ((bf16[4,16,32,1408]{3,2,1,0:T(8,128)(2,1)}), bf16[4,16,32,1408]{3,2,1,0:T(8,128)(2,1)}, u32[]{:S(2)}, u32[]{:S(2)}) async-start(bf16[4,16,32,1408]{3,2,1,0:T(8,128)(2,1)} %stack.30), calls=%async_computation.2 | async-start | bytes 11534336 | tf_op jit(solution)/shard_map/all_to_all | solution.py:42
  105.0 118.6 %copy-start.3 = (bf16[128,1,128]{2,0,1:T(8,128)(2,1)S(1)}, bf16[128,1,128]{2,0,1:T(8,128)(2,1)}, u32[]{:S(2)}) copy-start(bf16[128,1,128]{2,0,1:T(8,128)(2,1)} %param.18) | copy-start | bytes 98308
  243.0 9.8 %copy-start.2 = (bf16[704,32]{0,1:T(8,128)(2,1)S(1)}, bf16[704,32]{0,1:T(8,128)(2,1)}, u32[]{:S(2)}) copy-start(bf16[704,32]{0,1:T(8,128)(2,1)} %param.33) | copy-start | bytes 135172
  243.0 20.7 %copy-start.5 = (bf16[2048]{0:T(1024)(128)(2,1)S(1)}, bf16[2048]{0:T(1024)(128)(2,1)}, u32[]{:S(2)}) copy-start(bf16[2048]{0:T(1024)(128)(2,1)} %param.26) | copy-start | bytes 12292
  243.0 20.7 %copy-start.6 = (bf16[2048]{0:T(1024)(128)(2,1)S(1)}, bf16[2048]{0:T(1024)(128)(2,1)}, u32[]{:S(2)}) copy-start(bf16[2048]{0:T(1024)(128)(2,1)} %param.27) | copy-start | bytes 12292
  243.0 58.5 %all-to-all-start = ((bf16[8,128,2048]{2,1,0:T(8,128)(2,1)}), bf16[8,128,2048]{2,1,0:T(8,128)(2,1)}, u32[]{:S(2)}, u32[]{:S(2)}) async-start(bf16[8,128,2048]{2,1,0:T(8,128)(2,1)} %broadcast_in_dim.5), calls=%async_computation | async-start | bytes 8388608 | tf_op jit(solution)/shard_map/all_to_all | solution.py:25
  252.8 75.0 %all-gather.5.cloned.1.call-start = ((), (), s32[]{:S(2)}) async-start(), calls=%async_computation.5 | async-start | bytes 3342336 | tf_op jit(solution)/shard_map/all_gather | solution.py:69
  270.5 34.3 %copy-start.1 = (bf16[128,2048]{1,0:T(8,128)(2,1)S(1)}, bf16[128,2048]{1,0:T(8,128)(2,1)}, u32[]{:S(2)}) copy-start(bf16[128,2048]{1,0:T(8,128)(2,1)} %param.17) | copy-start | bytes 1572868
  309.0 2.7 collective-permute-start
  310.3 4.8 %collective-permute-start.1 = (bf16[1,1408]{1,0:T(2,128)(2,1)S(1)}, bf16[1,1408]{1,0:T(2,128)(2,1)S(1)}, u32[]{:S(2)}, u32[]{:S(2)}) collective-permute-start(bf16[1,1408]{1,0:T(2,128)(2,1)S(1)} %get-tuple-element.9), channel_id=1, source_target_pairs={{8,0},{16,8},{24,16},{32,24},{40,32},{48,40},{56,48},{64,56},{72,6... | collective-permute-start | bytes 8456 | tf_op jit(solution)/shard_map/ppermute | solution.py:62
  315.2 30.2 %copy-start.7 = (bf16[2048]{0:T(1024)(128)(2,1)S(1)}, bf16[2048]{0:T(1024)(128)(2,1)}, u32[]{:S(2)}) copy-start(bf16[2048]{0:T(1024)(128)(2,1)} %param.28) | copy-start | bytes 12292
  331.7 23.0 %all-to-all-start.3 = ((bf16[8,16,2048]{2,1,0:T(8,128)(2,1)}), bf16[8,16,2048]{2,1,0:T(8,128)(2,1)S(1)}, u32[]{:S(2)}, u32[]{:S(2)}) async-start(bf16[8,16,2048]{2,1,0:T(8,128)(2,1)} %bitcast.17), calls=%async_computation.3 | async-start | bytes 1048576 | tf_op jit(solution)/shard_map/all_to_all | solution.py:81
Sparse Core Ops, SparseCore 0:
  11.8 207.3 all-gather.2
Sparse Core Ops, SparseCore 1:
  263.8 64.0 all-gather.4
